TPU v7x, 32 devices: a whole 2x2x4 slice. The times are simulated.
32 devices in a mesh: sp: 8 (over z, x), tp: 4 (over y, core).
Axes of the slice: x: 2, y: 2, z: 4, core: 2. Of those that a mesh axis runs over, the one named last changes fastest.
Arguments:
- inputs: bfloat16 [4096, 2048], P('sp', 'tp'), may hold values from -45 to 45
- norm_gain: float32 [3, 2048], replicated, may hold values from 0.1 to 1.9
- w_value: bfloat16 [3, 2048, 1024], P(None, 'sp', 'tp'), may hold values from -0.125 to 0.125
- w_gate: bfloat16 [3, 2048, 1024], P(None, 'sp', 'tp'), may hold values from -0.125 to 0.125
- conv_taps: float32 [3, 31, 1024], P(None, None, 'tp'), may hold values from -5 to 5
- ln_gain: float32 [3, 1024], P(None, 'tp'), may hold values from 0.1 to 1.9
- ln_bias: float32 [3, 1024], P(None, 'tp'), may hold values from -3 to 3
- w_out: bfloat16 [3, 1024, 2048], P(None, 'tp', 'sp'), may hold values from -0.1875 to 0.1875
Outputs:
- stream: bfloat16 [4096, 2048], P('sp', 'tp')
All inputs are finite; a program needn't handle non-finite values.
Results may differ from a plain program's by a relative error of at most 0.01.
Values may be sent and summed in bfloat16 or wider, within the bound.
A program may use at most 64 MiB of HBM per device.

v0:
```python
import jax
import jax.numpy as jnp
from jax import lax
from jax.sharding import PartitionSpec as P


def from_behind(block, axis, distance):
    devices = range(lax.axis_size(axis))
    route = [(i - distance, i) for i in devices if i - distance in devices]
    return lax.ppermute(block, axis, route)


def shards(inputs, norm_gain, w_value, w_gate, conv_taps, ln_gain, ln_bias, w_out):
    rows = inputs.shape[0]
    reach = conv_taps.shape[1] - 1
    layers = conv_taps.shape[0]
    channels = conv_taps.shape[2] * lax.axis_size("tp")
    whole_value, whole_gate, whole_out = (
        lax.all_gather(w_value, "sp", axis=1, tiled=True),
        lax.all_gather(w_gate, "sp", axis=1, tiled=True),
        lax.all_gather(w_out, "sp", axis=2, tiled=True),
    )
    stream = inputs
    for layer in range(layers):
        full_rows = lax.all_gather(stream, "tp", axis=1, tiled=True)
        xf = full_rows.astype(jnp.float32)
        meansq = jnp.mean(xf * xf, axis=1, keepdims=True)
        hidden = (xf * lax.rsqrt(meansq + 1e-06) * norm_gain[layer][None, :]).astype(jnp.bfloat16)
        value = jnp.dot(hidden, whole_value[layer], preferred_element_type=jnp.float32)
        gate = jnp.dot(hidden, whole_gate[layer], preferred_element_type=jnp.float32)
        glu = (value * jax.nn.sigmoid(gate)).astype(jnp.bfloat16)
        rim = from_behind(glu[rows - reach :], "sp", 1)
        padded = jnp.concatenate([rim, glu], axis=0)
        count = padded.shape[0] - reach
        filtered = jnp.zeros((count, glu.shape[1]), jnp.float32)
        for tap in range(reach + 1):
            filtered = filtered + conv_taps[layer, tap][None, :] * padded[tap : tap + count].astype(
                jnp.float32
            )
        total_sum, total_sq = lax.psum(
            (jnp.sum(filtered, axis=1), jnp.sum(filtered * filtered, axis=1)), "tp"
        )
        mean_val = (total_sum / channels)[:, None]
        var_val = (total_sq / channels)[:, None] - mean_val * mean_val
        normed = jax.nn.silu(
            (filtered - mean_val) * lax.rsqrt(var_val + 1e-06) * ln_gain[layer][None, :]
            + ln_bias[layer][None, :]
        ).astype(jnp.bfloat16)
        partial_out = jnp.dot(normed, whole_out[layer], preferred_element_type=jnp.float32)
        summed = lax.psum_scatter(
            partial_out.astype(jnp.bfloat16), "tp", scatter_dimension=1, tiled=True
        ).astype(jnp.float32)
        kept = stream.astype(jnp.float32)
        stream = (kept + summed).astype(jnp.bfloat16)
    return stream


def solution(mesh):
    in_specs = (
        P("sp", "tp"),
        P(),
        P(None, "sp", "tp"),
        P(None, "sp", "tp"),
        P(None, None, "tp"),
        P(None, "tp"),
        P(None, "tp"),
        P(None, "tp", "sp"),
    )
    out_specs = P("sp", "tp")
    return jax.shard_map(shards, mesh=mesh, in_specs=in_specs, out_specs=out_specs, check_vma=False)
```

profile of v0, /device:TPU:0, one launch (start us, length us, event | category | flops | bytes accessed | tf_op | source)
XLA Modules:
  0.0 422.9 jit_solution(3484355526385756584)
XLA Ops:
  13.1 21.1 %all-gather.7.cloned.1.call-done = bf16[512,2048]{1,0:T(8,128)(2,1)} async-done(((bf16[512,512]{1,0:T(8,128)(2,1)}), bf16[512,2048]{1,0:T(8,128)(2,1)}) %all-gather.7.cloned.1.call-update) | async-done | bytes 2097168 | tf_op jit(solution)/shard_map/all_gather | solution.py:25
  36.3 60.1 %all-gather.11.cloned.1.call-done = bf16[3,2048,256]{2,1,0:T(8,128)(2,1)} async-done(((bf16[3,256,256]{2,1,0:T(8,128)(2,1)}), bf16[3,2048,256]{2,1,0:T(8,128)(2,1)}) %all-gather.11.cloned.1.call-update) | async-done | bytes 3145744 | tf_op jit(solution)/shard_map/all_gather | solution.py:20
  96.4 2.8 fusion.17
  99.2 58.1 %all-gather.9.cloned.1.call-done = bf16[3,2048,256]{2,1,0:T(8,128)(2,1)} async-done(((bf16[3,256,256]{2,1,0:T(8,128)(2,1)}), bf16[3,2048,256]{2,1,0:T(8,128)(2,1)}) %all-gather.9.cloned.1.call-update) | async-done | bytes 3145744 | tf_op jit(solution)/shard_map/all_gather | solution.py:19
  159.4 2.5 collective-permute-start
  163.3 2.4 fusion.134
  165.7 5.7 %all-reduce.2 = (f32[512]{0:T(512)S(1)}, f32[512]{0:T(512)S(1)}) all-reduce(f32[512]{0:T(512)S(1)} %get-tuple-element.10, f32[512]{0:T(512)S(1)} %get-tuple-element.9), channel_id=1, replica_groups=mesh['sp'=8,'tp'=4] {'tp'}, use_global_device_ids=true, to_apply=%region_4.0 | all-reduce | flops 1024 | bytes 8192 | tf_op jit(solution)/shard_map/psum | solution.py:40
  171.4 49.2 %all-gather.13.cloned.1.call-done = bf16[3,256,2048]{2,1,0:T(8,128)(2,1)} async-done(((bf16[3,256,256]{2,1,0:T(8,128)(2,1)}), bf16[3,256,2048]{2,1,0:T(8,128)(2,1)}) %all-gather.13.cloned.1.call-update) | async-done | bytes 3145744 | tf_op jit(solution)/shard_map/all_gather | solution.py:21
  220.6 3.4 convolution_convert_fusion.2
  224.1 29.5 %reduce-scatter.4.cloned.1.call-done = bf16[512,512]{1,0:T(8,128)(2,1)} async-done(((bf16[512,2048]{1,0:T(8,128)(2,1)}), bf16[512,512]{1,0:T(8,128)(2,1)}) %reduce-scatter.4.cloned.1.call-update) | async-done | bytes 524304 | tf_op jit(solution)/shard_map/reduce_scatter | solution.py:50
  255.6 22.6 %all-gather.15.cloned.1.call-done = bf16[512,2048]{1,0:T(8,128)(2,1)} async-done(((bf16[512,512]{1,0:T(8,128)(2,1)}), bf16[512,2048]{1,0:T(8,128)(2,1)}) %all-gather.15.cloned.1.call-update) | async-done | bytes 2097168 | tf_op jit(solution)/shard_map/all_gather | solution.py:25
  280.4 2.8 fusion.14
  285.2 3.4 collective-permute-start.1
  290.0 2.4 fusion.133
  292.4 6.0 %all-reduce.1 = (f32[512]{0:T(512)S(1)}, f32[512]{0:T(512)S(1)}) all-reduce(f32[512]{0:T(512)S(1)} %get-tuple-element.8, f32[512]{0:T(512)S(1)} %get-tuple-element.7), channel_id=1, replica_groups=mesh['sp'=8,'tp'=4] {'tp'}, use_global_device_ids=true, to_apply=%region_10.11 | all-reduce | flops 1024 | bytes 8192 | tf_op jit(solution)/shard_map/psum | solution.py:40
  298.4 3.4 convolution_convert_fusion.1
  301.9 32.1 %reduce-scatter.6.cloned.1.call-done = bf16[512,512]{1,0:T(8,128)(2,1)} async-done(((bf16[512,2048]{1,0:T(8,128)(2,1)}), bf16[512,512]{1,0:T(8,128)(2,1)}) %reduce-scatter.6.cloned.1.call-update) | async-done | bytes 524304 | tf_op jit(solution)/shard_map/reduce_scatter | solution.py:50
  336.0 22.7 %all-gather.17.cloned.1.call-done = bf16[512,2048]{1,0:T(8,128)(2,1)} async-done(((bf16[512,512]{1,0:T(8,128)(2,1)}), bf16[512,2048]{1,0:T(8,128)(2,1)}) %all-gather.17.cloned.1.call-update) | async-done | bytes 2097168 | tf_op jit(solution)/shard_map/all_gather | solution.py:25
  360.8 2.8 fusion.11
  365.6 3.6 collective-permute-start.2
  370.4 2.4 fusion.132
  372.8 5.9 %all-reduce = (f32[512]{0:T(512)S(1)}, f32[512]{0:T(512)S(1)}) all-reduce(f32[512]{0:T(512)S(1)} %get-tuple-element.6, f32[512]{0:T(512)S(1)} %get-tuple-element.5), channel_id=1, replica_groups=mesh['sp'=8,'tp'=4] {'tp'}, use_global_device_ids=true, to_apply=%region_16.17 | all-reduce | flops 1024 | bytes 8192 | tf_op jit(solution)/shard_map/psum | solution.py:40
  378.8 3.4 convolution_convert_fusion
  382.2 32.1 %reduce-scatter.8.cloned.1.call-done = bf16[512,512]{1,0:T(8,128)(2,1)} async-done(((bf16[512,2048]{1,0:T(8,128)(2,1)}), bf16[512,512]{1,0:T(8,128)(2,1)}) %reduce-scatter.8.cloned.1.call-update) | async-done | bytes 524304 | tf_op jit(solution)/shard_map/reduce_scatter | solution.py:50
  (63 shorter events, 29.1 us)
Async XLA Ops:
  6.5 27.7 %all-gather.7.cloned.1.call-start = ((), (), s32[]{:S(2)}) async-start(), calls=%async_computation.3 | async-start | bytes 2621440 | tf_op jit(solution)/shard_map/all_gather | solution.py:25
  7.3 89.2 %all-gather.11.cloned.1.call-start = ((), (), s32[]{:S(2)}) async-start(), calls=%async_computation.5 | async-start | bytes 3538944 | tf_op jit(solution)/shard_map/all_gather | solution.py:20
  8.0 149.3 %all-gather.9.cloned.1.call-start = ((), (), s32[]{:S(2)}) async-start(), calls=%async_computation.4 | async-start | bytes 3538944 | tf_op jit(solution)/shard_map/all_gather | solution.py:19
  8.7 211.9 %all-gather.13.cloned.1.call-start = ((), (), s32[]{:S(2)}) async-start(), calls=%async_computation.6 | async-start | bytes 3538944 | tf_op jit(solution)/shard_map/all_gather | solution.py:21
  9.3 244.2 %reduce-scatter.4.cloned.1.call-start = ((), (), s32[]{:S(2)}) async-start(), calls=%async_computation.7 | async-start | bytes 2621440 | tf_op jit(solution)/shard_map/reduce_scatter | solution.py:50
  96.4 60.9 %copy-start.3 = (bf16[512,2048]{1,0:T(8,128)(2,1)S(1)}, bf16[512,2048]{1,0:T(8,128)(2,1)}, u32[]{:S(2)}) copy-start(bf16[512,2048]{1,0:T(8,128)(2,1)} %all-gather.7.cloned.1.call-done) | copy-start | bytes 6291460
  99.2 62.6 %copy-start.7 = (f32[3,256]{1,0:T(4,128)S(1)}, f32[3,256]{1,0:T(4,128)}, u32[]{:S(2)}) copy-start(f32[3,256]{1,0:T(4,128)} %param.14) | copy-start | bytes 9220
  159.4 3.9 collective-permute-start
  220.6 33.0 %copy-start.2 = (bf16[512,512]{1,0:T(8,128)(2,1)S(1)}, bf16[512,512]{1,0:T(8,128)(2,1)}, u32[]{:S(2)}) copy-start(bf16[512,512]{1,0:T(8,128)(2,1)} %param.8) | copy-start | bytes 1572868
  224.0 31.6 %copy-start.6 = (f32[3,31,256]{2,1,0:T(8,128)S(1)}, f32[3,31,256]{2,1,0:T(8,128)}, u32[]{:S(2)}) copy-start(f32[3,31,256]{2,1,0:T(8,128)} %param.12) | copy-start | bytes 285700
  224.0 54.3 %all-gather.15.cloned.1.call-start = ((), (), s32[]{:S(2)}) async-start(), calls=%async_computation.8 | async-start | bytes 2621440 | tf_op jit(solution)/shard_map/all_gather | solution.py:25
  255.6 78.4 %reduce-scatter.6.cloned.1.call-start = ((), (), s32[]{:S(2)}) async-start(), calls=%async_computation.9 | async-start | bytes 2621440 | tf_op jit(solution)/shard_map/reduce_scatter | solution.py:50
  280.4 2.8 copy-start.4
  285.2 4.8 %collective-permute-start.1 = (bf16[30,256]{1,0:T(8,128)(2,1)S(1)}, bf16[30,256]{1,0:T(8,128)(2,1)S(1)}, u32[]{:S(2)}, u32[]{:S(2)}) collective-permute-start(bf16[30,256]{1,0:T(8,128)(2,1)S(1)} %slice.880), channel_id=1, source_target_pairs={{0,4},{4,8},{8,12},{12,16},{16,20},{20,24},{24,28},{1,5},{5,9},{9,... | collective-permute-start | bytes 46088 | tf_op jit(solution)/shard_map/ppermute | solution.py:10
  298.4 35.5 %copy-start = (bf16[512,512]{1,0:T(8,128)(2,1)S(1)}, bf16[512,512]{1,0:T(8,128)(2,1)}, u32[]{:S(2)}) copy-start(bf16[512,512]{1,0:T(8,128)(2,1)} %add_convert_fusion.2) | copy-start | bytes 1572868
  301.8 56.8 %all-gather.17.cloned.1.call-start = ((), (), s32[]{:S(2)}) async-start(), calls=%async_computation.10 | async-start | bytes 2621440 | tf_op jit(solution)/shard_map/all_gather | solution.py:25
  336.0 78.4 %reduce-scatter.8.cloned.1.call-start = ((), (), s32[]{:S(2)}) async-start(), calls=%async_computation.11 | async-start | bytes 2621440 | tf_op jit(solution)/shard_map/reduce_scatter | solution.py:50
  360.8 2.8 copy-start.5
  365.6 4.8 %collective-permute-start.2 = (bf16[30,256]{1,0:T(8,128)(2,1)S(1)}, bf16[30,256]{1,0:T(8,128)(2,1)S(1)}, u32[]{:S(2)}, u32[]{:S(2)}) collective-permute-start(bf16[30,256]{1,0:T(8,128)(2,1)S(1)} %slice.942), channel_id=1, source_target_pairs={{0,4},{4,8},{8,12},{12,16},{16,20},{20,24},{24,28},{1,5},{5,9},{9,... | collective-permute-start | bytes 46088 | tf_op jit(solution)/shard_map/ppermute | solution.py:10
  378.8 35.6 %copy-start.1 = (bf16[512,512]{1,0:T(8,128)(2,1)S(1)}, bf16[512,512]{1,0:T(8,128)(2,1)}, u32[]{:S(2)}) copy-start(bf16[512,512]{1,0:T(8,128)(2,1)} %add_convert_fusion.1) | copy-start | bytes 1572868
Sparse Core Ops, SparseCore 0:
  8.9 25.2 all-gather.6
  36.4 60.0 all-gather.10
  98.6 58.6 all-gather.8
  159.2 61.3 all-gather.12
  224.1 29.3 reduce-scatter.3
  255.7 22.5 all-gather.14
  302.0 31.9 reduce-scatter.5
  336.1 22.5 all-gather.16
  382.4 31.9 reduce-scatter.7
where the time goes:
time: 424 us; the launch traced here: 423 us
  waiting for transfers between devices  334 us (79%)
  matrix products  24.6 us (6%)
  other arithmetic  19.5 us (5%)
  blocking collectives  17.6 us (4%)
  between operations  13.4 us (3%)
  starting transfers between devices  9.7 us (2%)
    reduce_scatter x3, waiting for transfers between devices, shards(): lax.psum_scatter(partial_out.astype(jnp.bfloat16), 'tp', scatter_dimensio...  93.7 us
    all_gather x3, waiting for transfers between devices, shards(): full_rows = lax.all_gather(stream, 'tp', axis=1, tiled=True)  66.4 us
    all_gather x1, waiting for transfers between devices, shards(): lax.all_gather(w_gate, 'sp', axis=1, tiled=True)  60.1 us
    all_gather x1, waiting for transfers between devices, shards(): lax.all_gather(w_value, 'sp', axis=1, tiled=True)  58.1 us
    all_gather x1, waiting for transfers between devices, shards(): lax.all_gather(w_out, 'sp', axis=2, tiled=True)  49.2 us
    psum x3, blocking collectives, shards(): lax.psum((jnp.sum(filtered, axis=1), jnp.sum(filtered * filtered, axis=1)...  17.6 us
    dot_general x3, matrix products, shards(): jnp.dot(normed, whole_out[layer], preferred_element_type=jnp.float32)  10.2 us
    ppermute x3, starting transfers between devices, from_behind(): return lax.ppermute(block, axis, route)  9.38 us
  transfers between devices with their start and end apart: 12, of which 12 were waited for; matrix products, arithmetic and copies ran while one was open for 3% of the time, Pallas kernels for 0%

commit v1 on v0

--- a/solution.py
+++ b/solution.py
@@ -22,7 +22,13 @@
     )
     stream = inputs
     for layer in range(layers):
-        full_rows = lax.all_gather(stream, "tp", axis=1, tiled=True)
+        size = lax.axis_size("tp")
+        moving, parts = (stream, [stream])
+        for _ in range(size - 1):
+            moving = lax.ppermute(moving, "tp", [(i_2, (i_2 + 1) % size) for i_2 in range(size)])
+            parts.insert(0, moving)
+        line = jnp.concatenate(parts, axis=1)
+        full_rows = jnp.roll(line, (lax.axis_index("tp") + 1) * stream.shape[1], axis=1)
         xf = full_rows.astype(jnp.float32)
         meansq = jnp.mean(xf * xf, axis=1, keepdims=True)
         hidden = (xf * lax.rsqrt(meansq + 1e-06) * norm_gain[layer][None, :]).astype(jnp.bfloat16)

time: 424 us -> 410 us (0.967)
  waiting for transfers between devices: 334 us -> 313 us
  other arithmetic: 19.5 us -> 28.8 us
    ppermute x0 -> x9, waiting for transfers between devices: none -> 74.1 us  [shards(): lax.ppermute(moving, 'tp', [(i_2, (i_2 + 1) % size) for i_2 in range(size)])]
    all_gather x3 -> x0, waiting for transfers between devices: 66.4 us -> none  [shards(): full_rows = lax.all_gather(stream, 'tp', axis=1, tiled=True)]
    all_gather x1, waiting for transfers between devices: 60.1 us -> 30.8 us  [shards(): lax.all_gather(w_gate, 'sp', axis=1, tiled=True)]
    reduce_sum x3, other arithmetic: 6.22 us -> 17.2 us  [shards(): meansq = jnp.mean(xf * xf, axis=1, keepdims=True)]
  transfers between devices with their start and end apart: 12 -> 18, of which waited for: 12 -> 18; matrix products, arithmetic and copies ran while one was open for 3% -> 4% of each run, Pallas kernels for 0% -> 0%
where the time goes in v1:
time: 410 us; the launch traced here: 409 us
  waiting for transfers between devices  313 us (76%)
  other arithmetic  28.8 us (7%)
  matrix products  22.2 us (5%)
  blocking collectives  17.6 us (4%)
  between operations  13.7 us (3%)
  starting transfers between devices  10.3 us (3%)
    reduce_scatter x3, waiting for transfers between devices, shards(): lax.psum_scatter(partial_out.astype(jnp.bfloat16), 'tp', scatter_dimensio...  93.7 us
    ppermute x9, waiting for transfers between devices, shards(): lax.ppermute(moving, 'tp', [(i_2, (i_2 + 1) % size) for i_2 in range(size)])  74.1 us
    all_gather x1, waiting for transfers between devices, shards(): lax.all_gather(w_value, 'sp', axis=1, tiled=True)  58.9 us
    all_gather x1, waiting for transfers between devices, shards(): lax.all_gather(w_out, 'sp', axis=2, tiled=True)  49.4 us
    all_gather x1, waiting for transfers between devices, shards(): lax.all_gather(w_gate, 'sp', axis=1, tiled=True)  30.8 us
    psum x3, blocking collectives, shards(): lax.psum((jnp.sum(filtered, axis=1), jnp.sum(filtered * filtered, axis=1)...  17.6 us
    reduce_sum x3, other arithmetic, shards(): meansq = jnp.mean(xf * xf, axis=1, keepdims=True)  17.2 us
    dot_general x3, matrix products, shards(): jnp.dot(normed, whole_out[layer], preferred_element_type=jnp.float32)  10.1 us
  transfers between devices with their start and end apart: 18, of which 18 were waited for; matrix products, arithmetic and copies ran while one was open for 4% of the time, Pallas kernels for 0%

profile of v1, /device:TPU:0, one launch (start us, length us, event | category | flops | bytes accessed | tf_op | source)
XLA Modules:
  0.0 409.4 jit_solution(12010405297522412371)
XLA Ops:
  9.3 9.0 %collective-permute-done = bf16[512,512]{1,0:T(8,128)(2,1)S(1)} collective-permute-done((bf16[512,512]{1,0:T(8,128)(2,1)}, bf16[512,512]{1,0:T(8,128)(2,1)S(1)}, u32[]{:S(2)}, u32[]{:S(2)}) %collective-permute-start) | collective-permute-done | bytes 524320 | tf_op jit(solution)/shard_map/ppermute | solution.py:28
  20.5 6.5 %collective-permute-done.1 = bf16[512,512]{1,0:T(8,128)(2,1)S(1)} collective-permute-done((bf16[512,512]{1,0:T(8,128)(2,1)S(1)}, bf16[512,512]{1,0:T(8,128)(2,1)S(1)}, u32[]{:S(2)}, u32[]{:S(2)}) %collective-permute-start.1) | collective-permute-done | bytes 524320 | tf_op jit(solution)/shard_map/ppermute | solution.py:28
  28.7 7.0 %collective-permute-done.2 = bf16[512,512]{1,0:T(8,128)(2,1)} collective-permute-done((bf16[512,512]{1,0:T(8,128)(2,1)S(1)}, bf16[512,512]{1,0:T(8,128)(2,1)}, u32[]{:S(2)}, u32[]{:S(2)}) %collective-permute-start.2) | collective-permute-done | bytes 524320 | tf_op jit(solution)/shard_map/ppermute | solution.py:28
  35.7 5.8 %fusion = (f32[512]{0:T(512)S(1)}, bf16[512,2048]{1,0:T(8,128)(2,1)S(1)}) fusion(s32[]{:T(128)S(6)} %select_n.15, bf16[512,512]{1,0:T(8,128)(2,1)} %param.10, bf16[512,512]{1,0:T(8,128)(2,1)S(1)} %collective-permute-done, bf16[512,512]{1,0:T(8,128)(2,1)S(1)} %collective-permute-done.1, bf16[512,512]{1,0:T(8,128)(2,1)} %collective-permute-done.2), kind=kLoop, calls=%fused_computation.6 | loop fusion | flops 19922432 | bytes 4196356 | tf_op jit(solution)/shard_map/reduce_sum | solution.py:33
  41.5 30.8 %all-gather.6.cloned.1.call-done = bf16[3,2048,256]{2,1,0:T(8,128)(2,1)} async-done(((bf16[3,256,256]{2,1,0:T(8,128)(2,1)}), bf16[3,2048,256]{2,1,0:T(8,128)(2,1)}) %all-gather.6.cloned.1.call-update) | async-done | bytes 3145744 | tf_op jit(solution)/shard_map/all_gather | solution.py:20
  74.3 58.9 %all-gather.4.cloned.1.call-done = bf16[3,2048,256]{2,1,0:T(8,128)(2,1)} async-done(((bf16[3,256,256]{2,1,0:T(8,128)(2,1)}), bf16[3,2048,256]{2,1,0:T(8,128)(2,1)}) %all-gather.4.cloned.1.call-update) | async-done | bytes 3145744 | tf_op jit(solution)/shard_map/all_gather | solution.py:19
  141.5 5.7 %all-reduce.2 = (f32[512]{0:T(512)S(1)}, f32[512]{0:T(512)S(1)}) all-reduce(f32[512]{0:T(512)S(1)} %get-tuple-element.11, f32[512]{0:T(512)S(1)} %get-tuple-element.10), channel_id=1, replica_groups=mesh['sp'=8,'tp'=4] {'tp'}, use_global_device_ids=true, to_apply=%region_4.6 | all-reduce | flops 1024 | bytes 8192 | tf_op jit(solution)/shard_map/psum | solution.py:46
  147.2 49.4 %all-gather.8.cloned.1.call-done = bf16[3,256,2048]{2,1,0:T(8,128)(2,1)} async-done(((bf16[3,256,256]{2,1,0:T(8,128)(2,1)}), bf16[3,256,2048]{2,1,0:T(8,128)(2,1)}) %all-gather.8.cloned.1.call-update) | async-done | bytes 3145744 | tf_op jit(solution)/shard_map/all_gather | solution.py:21
  196.6 3.4 convolution_convert_fusion.2
  200.1 29.5 %reduce-scatter.4.cloned.1.call-done = bf16[512,512]{1,0:T(8,128)(2,1)} async-done(((bf16[512,2048]{1,0:T(8,128)(2,1)}), bf16[512,512]{1,0:T(8,128)(2,1)}) %reduce-scatter.4.cloned.1.call-update) | async-done | bytes 524304 | tf_op jit(solution)/shard_map/reduce_scatter | solution.py:56
  230.8 8.6 %collective-permute-done.4 = bf16[512,512]{1,0:T(8,128)(2,1)S(1)} collective-permute-done((bf16[512,512]{1,0:T(8,128)(2,1)S(1)}, bf16[512,512]{1,0:T(8,128)(2,1)S(1)}, u32[]{:S(2)}, u32[]{:S(2)}) %collective-permute-start.4) | collective-permute-done | bytes 524320 | tf_op jit(solution)/shard_map/ppermute | solution.py:28
  239.4 8.6 %collective-permute-done.5 = bf16[512,512]{1,0:T(8,128)(2,1)S(1)} collective-permute-done((bf16[512,512]{1,0:T(8,128)(2,1)S(1)}, bf16[512,512]{1,0:T(8,128)(2,1)S(1)}, u32[]{:S(2)}, u32[]{:S(2)}) %collective-permute-start.5) | collective-permute-done | bytes 524320 | tf_op jit(solution)/shard_map/ppermute | solution.py:28
  248.0 8.6 %collective-permute-done.6 = bf16[512,512]{1,0:T(8,128)(2,1)S(1)} collective-permute-done((bf16[512,512]{1,0:T(8,128)(2,1)S(1)}, bf16[512,512]{1,0:T(8,128)(2,1)S(1)}, u32[]{:S(2)}, u32[]{:S(2)}) %collective-permute-start.6) | collective-permute-done | bytes 524320 | tf_op jit(solution)/shard_map/ppermute | solution.py:28
  256.6 5.7 %fusion.3 = (f32[512]{0:T(512)S(1)}, bf16[512,2048]{1,0:T(8,128)(2,1)S(1)}) fusion(s32[]{:T(128)S(6)} %select_n.15, bf16[512,512]{1,0:T(8,128)(2,1)S(1)} %add_convert_fusion.2, bf16[512,512]{1,0:T(8,128)(2,1)S(1)} %collective-permute-done.4, bf16[512,512]{1,0:T(8,128)(2,1)S(1)} %collective-permute-done.5, bf16[512,512]{1,0:T(8,128)(2,1)S(1)} %collective-permute-done.6), kind=kLoop, calls=%fused_computation.9 | loop fusion | flops 19922432 | bytes 4196356 | tf_op jit(solution)/shard_map/reduce_sum | solution.py:33
  273.6 6.0 %all-reduce.1 = (f32[512]{0:T(512)S(1)}, f32[512]{0:T(512)S(1)}) all-reduce(f32[512]{0:T(512)S(1)} %get-tuple-element.9, f32[512]{0:T(512)S(1)} %get-tuple-element.8), channel_id=1, replica_groups=mesh['sp'=8,'tp'=4] {'tp'}, use_global_device_ids=true, to_apply=%region_10.12 | all-reduce | flops 1024 | bytes 8192 | tf_op jit(solution)/shard_map/psum | solution.py:46
  283.0 32.1 %reduce-scatter.6.cloned.1.call-done = bf16[512,512]{1,0:T(8,128)(2,1)} async-done(((bf16[512,2048]{1,0:T(8,128)(2,1)}), bf16[512,512]{1,0:T(8,128)(2,1)}) %reduce-scatter.6.cloned.1.call-update) | async-done | bytes 524304 | tf_op jit(solution)/shard_map/reduce_scatter | solution.py:56
  316.3 8.6 %collective-permute-done.8 = bf16[512,512]{1,0:T(8,128)(2,1)S(1)} collective-permute-done((bf16[512,512]{1,0:T(8,128)(2,1)S(1)}, bf16[512,512]{1,0:T(8,128)(2,1)S(1)}, u32[]{:S(2)}, u32[]{:S(2)}) %collective-permute-start.8) | collective-permute-done | bytes 524320 | tf_op jit(solution)/shard_map/ppermute | solution.py:28
  324.9 8.6 %collective-permute-done.9 = bf16[512,512]{1,0:T(8,128)(2,1)S(1)} collective-permute-done((bf16[512,512]{1,0:T(8,128)(2,1)S(1)}, bf16[512,512]{1,0:T(8,128)(2,1)S(1)}, u32[]{:S(2)}, u32[]{:S(2)}) %collective-permute-start.9) | collective-permute-done | bytes 524320 | tf_op jit(solution)/shard_map/ppermute | solution.py:28
  333.5 8.6 %collective-permute-done.10 = bf16[512,512]{1,0:T(8,128)(2,1)S(1)} collective-permute-done((bf16[512,512]{1,0:T(8,128)(2,1)S(1)}, bf16[512,512]{1,0:T(8,128)(2,1)S(1)}, u32[]{:S(2)}, u32[]{:S(2)}) %collective-permute-start.10) | collective-permute-done | bytes 524320 | tf_op jit(solution)/shard_map/ppermute | solution.py:28
  342.1 5.7 %fusion.6 = (f32[512]{0:T(512)S(1)}, bf16[512,2048]{1,0:T(8,128)(2,1)S(1)}) fusion(s32[]{:T(128)S(6)} %select_n.15, bf16[512,512]{1,0:T(8,128)(2,1)S(1)} %add_convert_fusion.1, bf16[512,512]{1,0:T(8,128)(2,1)S(1)} %collective-permute-done.8, bf16[512,512]{1,0:T(8,128)(2,1)S(1)} %collective-permute-done.9, bf16[512,512]{1,0:T(8,128)(2,1)S(1)} %collective-permute-done.10), kind=kLoop, calls=%fused_computation.12 | loop fusion | flops 19922432 | bytes 4196356 | tf_op jit(solution)/shard_map/reduce_sum | solution.py:33
  351.9 3.6 collective-permute-start.11
  359.1 5.9 %all-reduce = (f32[512]{0:T(512)S(1)}, f32[512]{0:T(512)S(1)}) all-reduce(f32[512]{0:T(512)S(1)} %get-tuple-element.7, f32[512]{0:T(512)S(1)} %get-tuple-element.6), channel_id=1, replica_groups=mesh['sp'=8,'tp'=4] {'tp'}, use_global_device_ids=true, to_apply=%region_16.18 | all-reduce | flops 1024 | bytes 8192 | tf_op jit(solution)/shard_map/psum | solution.py:46
  365.1 3.4 convolution_convert_fusion
  368.5 32.1 %reduce-scatter.8.cloned.1.call-done = bf16[512,512]{1,0:T(8,128)(2,1)} async-done(((bf16[512,2048]{1,0:T(8,128)(2,1)}), bf16[512,512]{1,0:T(8,128)(2,1)}) %reduce-scatter.8.cloned.1.call-update) | async-done | bytes 524304 | tf_op jit(solution)/shard_map/reduce_scatter | solution.py:56
  (62 shorter events, 43.7 us)
Async XLA Ops:
  6.5 65.8 %all-gather.6.cloned.1.call-start = ((), (), s32[]{:S(2)}) async-start(), calls=%async_computation.4 | async-start | bytes 3538944 | tf_op jit(solution)/shard_map/all_gather | solution.py:20
  7.3 125.9 %all-gather.4.cloned.1.call-start = ((), (), s32[]{:S(2)}) async-start(), calls=%async_computation.3 | async-start | bytes 3538944 | tf_op jit(solution)/shard_map/all_gather | solution.py:19
  8.0 188.6 %all-gather.8.cloned.1.call-start = ((), (), s32[]{:S(2)}) async-start(), calls=%async_computation.5 | async-start | bytes 3538944 | tf_op jit(solution)/shard_map/all_gather | solution.py:21
  8.7 220.8 %reduce-scatter.4.cloned.1.call-start = ((), (), s32[]{:S(2)}) async-start(), calls=%async_computation.6 | async-start | bytes 2621440 | tf_op jit(solution)/shard_map/reduce_scatter | solution.py:56
  8.8 9.6 %collective-permute-start = (bf16[512,512]{1,0:T(8,128)(2,1)}, bf16[512,512]{1,0:T(8,128)(2,1)S(1)}, u32[]{:S(2)}, u32[]{:S(2)}) collective-permute-start(bf16[512,512]{1,0:T(8,128)(2,1)} %param.10), channel_id=1, source_target_pairs={{0,1},{1,2},{2,3},{3,0},{4,5},{5,6},{6,7},{7,4},{8,9},{9,10},{10,1... | collective-permute-start | bytes 1572872 | tf_op jit(solution)/shard_map/ppermute | solution.py:28
  18.4 8.6 %collective-permute-start.1 = (bf16[512,512]{1,0:T(8,128)(2,1)S(1)}, bf16[512,512]{1,0:T(8,128)(2,1)S(1)}, u32[]{:S(2)}, u32[]{:S(2)}) collective-permute-start(bf16[512,512]{1,0:T(8,128)(2,1)S(1)} %collective-permute-done), channel_id=1, source_target_pairs={{0,1},{1,2},{2,3},{3,0},{4,5},{5,6},{6,7},{7,4},{8,9},{9,10},{10,1... | collective-permute-start | bytes 1572872 | tf_op jit(solution)/shard_map/ppermute | solution.py:28
  27.0 8.7 %collective-permute-start.2 = (bf16[512,512]{1,0:T(8,128)(2,1)S(1)}, bf16[512,512]{1,0:T(8,128)(2,1)}, u32[]{:S(2)}, u32[]{:S(2)}) collective-permute-start(bf16[512,512]{1,0:T(8,128)(2,1)S(1)} %collective-permute-done.1), channel_id=1, source_target_pairs={{0,1},{1,2},{2,3},{3,0},{4,5},{5,6},{6,7},{7,4},{8,9},{9,10},{10,1... | collective-permute-start | bytes 1572872 | tf_op jit(solution)/shard_map/ppermute | solution.py:28
  74.3 63.4 %copy-start.2 = (f32[3,256]{1,0:T(4,128)S(1)}, f32[3,256]{1,0:T(4,128)}, u32[]{:S(2)}) copy-start(f32[3,256]{1,0:T(4,128)} %param.16) | copy-start | bytes 9220
  135.2 3.9 collective-permute-start.3
  196.6 33.0 %copy-start = (bf16[512,512]{1,0:T(8,128)(2,1)S(1)}, bf16[512,512]{1,0:T(8,128)(2,1)}, u32[]{:S(2)}) copy-start(bf16[512,512]{1,0:T(8,128)(2,1)} %param.10) | copy-start | bytes 1572868
  200.0 48.0 %copy-start.1 = (f32[3,31,256]{2,1,0:T(8,128)S(1)}, f32[3,31,256]{2,1,0:T(8,128)}, u32[]{:S(2)}) copy-start(f32[3,31,256]{2,1,0:T(8,128)} %param.14) | copy-start | bytes 285700
  200.0 115.0 %reduce-scatter.6.cloned.1.call-start = ((), (), s32[]{:S(2)}) async-start(), calls=%async_computation.7 | async-start | bytes 2621440 | tf_op jit(solution)/shard_map/reduce_scatter | solution.py:56
  230.7 8.7 %collective-permute-start.4 = (bf16[512,512]{1,0:T(8,128)(2,1)S(1)}, bf16[512,512]{1,0:T(8,128)(2,1)S(1)}, u32[]{:S(2)}, u32[]{:S(2)}) collective-permute-start(bf16[512,512]{1,0:T(8,128)(2,1)S(1)} %add_convert_fusion.2), channel_id=1, source_target_pairs={{0,1},{1,2},{2,3},{3,0},{4,5},{5,6},{6,7},{7,4},{8,9},{9,10},{10,1... | collective-permute-start | bytes 1572872 | tf_op jit(solution)/shard_map/ppermute | solution.py:28
  239.4 8.6 %collective-permute-start.5 = (bf16[512,512]{1,0:T(8,128)(2,1)S(1)}, bf16[512,512]{1,0:T(8,128)(2,1)S(1)}, u32[]{:S(2)}, u32[]{:S(2)}) collective-permute-start(bf16[512,512]{1,0:T(8,128)(2,1)S(1)} %collective-permute-done.4), channel_id=1, source_target_pairs={{0,1},{1,2},{2,3},{3,0},{4,5},{5,6},{6,7},{7,4},{8,9},{9,10},{10,1... | collective-permute-start | bytes 1572872 | tf_op jit(solution)/shard_map/ppermute | solution.py:28
  248.0 8.6 %collective-permute-start.6 = (bf16[512,512]{1,0:T(8,128)(2,1)S(1)}, bf16[512,512]{1,0:T(8,128)(2,1)S(1)}, u32[]{:S(2)}, u32[]{:S(2)}) collective-permute-start(bf16[512,512]{1,0:T(8,128)(2,1)S(1)} %collective-permute-done.5), channel_id=1, source_target_pairs={{0,1},{1,2},{2,3},{3,0},{4,5},{5,6},{6,7},{7,4},{8,9},{9,10},{10,1... | collective-permute-start | bytes 1572872 | tf_op jit(solution)/shard_map/ppermute | solution.py:28
  266.4 4.8 %collective-permute-start.7 = (bf16[30,256]{1,0:T(8,128)(2,1)S(1)}, bf16[30,256]{1,0:T(8,128)(2,1)S(1)}, u32[]{:S(2)}, u32[]{:S(2)}) collective-permute-start(bf16[30,256]{1,0:T(8,128)(2,1)S(1)} %slice.880), channel_id=1, source_target_pairs={{0,4},{4,8},{8,12},{12,16},{16,20},{20,24},{24,28},{1,5},{5,9},{9,... | collective-permute-start | bytes 46088 | tf_op jit(solution)/shard_map/ppermute | solution.py:10
  282.9 117.7 %reduce-scatter.8.cloned.1.call-start = ((), (), s32[]{:S(2)}) async-start(), calls=%async_computation.8 | async-start | bytes 2621440 | tf_op jit(solution)/shard_map/reduce_scatter | solution.py:56
  316.3 8.7 %collective-permute-start.8 = (bf16[512,512]{1,0:T(8,128)(2,1)S(1)}, bf16[512,512]{1,0:T(8,128)(2,1)S(1)}, u32[]{:S(2)}, u32[]{:S(2)}) collective-permute-start(bf16[512,512]{1,0:T(8,128)(2,1)S(1)} %add_convert_fusion.1), channel_id=1, source_target_pairs={{0,1},{1,2},{2,3},{3,0},{4,5},{5,6},{6,7},{7,4},{8,9},{9,10},{10,1... | collective-permute-start | bytes 1572872 | tf_op jit(solution)/shard_map/ppermute | solution.py:28
  324.9 8.6 %collective-permute-start.9 = (bf16[512,512]{1,0:T(8,128)(2,1)S(1)}, bf16[512,512]{1,0:T(8,128)(2,1)S(1)}, u32[]{:S(2)}, u32[]{:S(2)}) collective-permute-start(bf16[512,512]{1,0:T(8,128)(2,1)S(1)} %collective-permute-done.8), channel_id=1, source_target_pairs={{0,1},{1,2},{2,3},{3,0},{4,5},{5,6},{6,7},{7,4},{8,9},{9,10},{10,1... | collective-permute-start | bytes 1572872 | tf_op jit(solution)/shard_map/ppermute | solution.py:28
  333.5 8.6 %collective-permute-start.10 = (bf16[512,512]{1,0:T(8,128)(2,1)S(1)}, bf16[512,512]{1,0:T(8,128)(2,1)S(1)}, u32[]{:S(2)}, u32[]{:S(2)}) collective-permute-start(bf16[512,512]{1,0:T(8,128)(2,1)S(1)} %collective-permute-done.9), channel_id=1, source_target_pairs={{0,1},{1,2},{2,3},{3,0},{4,5},{5,6},{6,7},{7,4},{8,9},{9,10},{10,1... | collective-permute-start | bytes 1572872 | tf_op jit(solution)/shard_map/ppermute | solution.py:28
  351.9 4.8 %collective-permute-start.11 = (bf16[30,256]{1,0:T(8,128)(2,1)S(1)}, bf16[30,256]{1,0:T(8,128)(2,1)S(1)}, u32[]{:S(2)}, u32[]{:S(2)}) collective-permute-start(bf16[30,256]{1,0:T(8,128)(2,1)S(1)} %slice.942), channel_id=1, source_target_pairs={{0,4},{4,8},{8,12},{12,16},{16,20},{20,24},{24,28},{1,5},{5,9},{9,... | collective-permute-start | bytes 46088 | tf_op jit(solution)/shard_map/ppermute | solution.py:10
Sparse Core Ops, SparseCore 0:
  9.5 62.7 all-gather.5
  74.5 58.6 all-gather.3
  135.2 61.3 all-gather.7
  200.1 29.3 reduce-scatter.3
  283.0 31.9 reduce-scatter.5
  368.6 31.9 reduce-scatter.7
